TPU v7x, 32 devices: a whole 2x2x4 slice. The times are simulated.
32 devices in a mesh: row: 16 (over z, y, x), col: 2 (over core).
Axes of the slice: x: 2, y: 2, z: 4, core: 2. Of those that a mesh axis runs over, the one named last changes fastest.
Arguments:
- tokens: bfloat16 [2, 8192, 2048], P(None, 'row'), may hold values from -6 to 6
- w_value: bfloat16 [2048, 1024], P(None, 'col'), may hold values from -0.125 to 0.125
- w_first: bfloat16 [2048, 1024], P(None, 'col'), may hold values from -0.125 to 0.125
- w_second: bfloat16 [2048, 1024], P(None, 'col'), may hold values from -0.125 to 0.125
- short_taps: float32 [3, 3, 1024], P(None, None, 'col'), may hold values from -3.5 to 3.5
- filter_in: float32 [33, 64], replicated, may hold values from -2 to 2
- filter_mid: float32 [64, 64], replicated, may hold values from -1.5 to 1.5
- filter_out: float32 [64, 2, 2, 1024], P(None, None, None, 'col'), may hold values from -0.75 to 0.75
- decay_rate: float32 [1024], P('col'), may hold values from 0 to 1, as said below
- skip_gain: float32 [2, 1024], P(None, 'col'), may hold values from -4 to 4
- w_output: bfloat16 [1024, 2048], P(None, 'col'), may hold values from -0.1875 to 0.1875
Outputs:
- mixed_out: bfloat16 [2, 8192, 2048], P(None, 'row', 'col')
Inputs may be any that keep to these rules, and one draw needn't show every extreme that they name: `decay_rate`: Per-position decay rates of the channels' filters; all positive.
All inputs are finite; a program needn't handle non-finite values.
Results may differ from a plain program's by a relative error of at most 0.007.
Values may be sent and summed in bfloat16 or wider, within the bound.
A program may use at most 128 MiB of HBM per device.

v0:
```python
import functools
import math

import jax
import jax.numpy as jnp
import numpy as np
from jax import lax
from jax.experimental import pallas as pl
from jax.experimental.pallas import tpu as pltpu
from jax.sharding import PartitionSpec as P

LANES = 128
f32 = jnp.float32
bf16 = jnp.bfloat16
highest = lax.Precision.HIGHEST


def split_table(table):
    table = np.asarray(table, np.float32)
    high = table.astype(bf16)
    low = (table - high.astype(np.float32)).astype(bf16)
    return np.stack([high, low])


def transform_tables(full_length):
    rows = full_length // LANES
    half = rows // 2
    r = np.arange(rows)
    q = np.arange(LANES)
    angle_rows = 2.0 * np.pi * ((r[:, None] * r[None, :]) % rows) / rows
    angle_cols = 2.0 * np.pi * ((q[:, None] * q[None, :]) % LANES) / LANES
    angle_turn = 2.0 * np.pi * ((r[:, None] * q[None, :]) % full_length) / full_length
    c1, s1 = np.cos(angle_rows), np.sin(angle_rows)
    c2, s2 = np.cos(angle_cols), np.sin(angle_cols)
    real_rows = split_table(np.concatenate([c1, -s1], 0))
    pair_rows = np.block([[c1[:, :half], s1[:, :half]], [-s1[:, :half], c1[:, :half]]])
    fore_cols = np.block([[c2, -s2], [s2, c2]])
    back_cols = np.block([[c2, s2], [-s2, c2]])
    turn = np.stack([np.cos(angle_turn), np.sin(angle_turn)]).astype(np.float32)
    return (
        real_rows,
        split_table(pair_rows),
        split_table(pair_rows.T),
        split_table(fore_cols),
        split_table(back_cols),
        turn,
    )


def dot(a, b):
    return jnp.dot(a, b, preferred_element_type=f32)


def wave(x):
    turns = jnp.floor(x * (1.0 / math.pi) + 0.5)
    r = x - turns * 3.140625
    r = r - turns * 9.67502593994140625e-4
    r = r - turns * 1.509957990978376e-7
    odd = turns - 2.0 * jnp.floor(turns * 0.5)
    r = r * (1.0 - 2.0 * odd)
    q = r * r
    p = -2.5052108e-8
    for coef in (2.7557319e-6, -1.9841270e-4, 8.3333333e-3, -1.6666667e-1):
        p = p * q + coef
    return r + r * q * p


def filter_kernel(
    bands, length, sig_batch, chunk, steps, w_in, w_mid, w_out, rates, rows_ref, cols_ref, turn_ref,
    spec_ref, line_ref, power_ref
):
    i = pl.program_id(0)
    sigs = w_out.shape[1]
    full = 2 * length
    n1_count = full // LANES

    @pl.when(i == 0)
    def _():
        power_ref[...] = jnp.zeros_like(power_ref)

    @pl.when(i < steps)
    def _():
        feat_rows = w_in.shape[1]
        n = i * chunk + lax.broadcasted_iota(jnp.int32, (1, chunk), 1)
        m = jnp.where(n < length, n, full - n).astype(f32)
        row = lax.broadcasted_iota(jnp.int32, (feat_rows, 1), 0)
        band = jnp.where(row <= bands, row - 1, row - 1 - bands).astype(f32)
        freq = 0.0001 + (bands - 1 - 0.0001) / (bands - 1) * band
        phase = jnp.where(row <= bands, 0.5 * math.pi, math.pi).astype(f32)
        angle = (2.0 * math.pi / length * m) * freq + phase
        feats = jnp.where(
            row == 0, m * (1.0 / (length - 1)), jnp.where(row <= 2 * bands, wave(angle), 0.0)
        )
        hidden = wave(jnp.dot(w_in[...], feats, precision=highest, preferred_element_type=f32))
        hidden = wave(jnp.dot(w_mid[...], hidden, precision=highest, preferred_element_type=f32))
        side = i // (steps // 2)
        shaped = jnp.dot(w_out[side], hidden, precision=highest, preferred_element_type=f32)
        damp = jnp.exp(-rates[:, 0:1] * m)
        damp = jnp.where(n == length, 0.0, damp)
        shaped = shaped * jnp.concatenate([damp, damp], axis=0)
        power = power_ref[...]
        for j in range(chunk // LANES):
            tile = shaped[:, j * LANES : (j + 1) * LANES]
            power = power + tile * tile
            at = pl.multiple_of((i * (chunk // LANES) + j) * sigs, sigs)
            line_ref[pl.ds(at, sigs), :] = tile
        power_ref[...] = power

    @pl.when(i == steps)
    def _():
        total = jnp.sum(power_ref[...], axis=1, keepdims=True)
        power_ref[...] = jnp.broadcast_to(lax.rsqrt(total + 1e-6) * (1.0 / full), power_ref.shape)

    @pl.when(i >= steps)
    def _():
        c, s = turn_ref[0], turn_ref[1]
        first = (i - steps) * sig_batch
        parts = []
        for b in range(sig_batch):
            line = line_ref[pl.ds(first + b, n1_count, stride=sigs), :]
            parts.append(line * power_ref[pl.ds(first + b, 1), :])
        x = jnp.concatenate(parts, axis=1)
        hi = x.astype(bf16)
        lo = (x - hi.astype(f32)).astype(bf16)
        a = dot(rows_ref[0], hi) + dot(rows_ref[1], hi) + dot(rows_ref[0], lo)
        turned = []
        for b in range(sig_batch):
            ar = a[:n1_count, b * LANES : (b + 1) * LANES]
            ai = a[n1_count:, b * LANES : (b + 1) * LANES]
            turned.append(jnp.concatenate([ar * c + ai * s, ai * c - ar * s], axis=1))
        t = jnp.concatenate(turned, axis=0)
        hi = t.astype(bf16)
        lo = (t - hi.astype(f32)).astype(bf16)
        spec = dot(hi, cols_ref[0]) + dot(hi, cols_ref[1]) + dot(lo, cols_ref[0])
        spec_ref[...] = spec.reshape(spec_ref.shape)


def make_spectrum(length, filter_in, filter_mid, out_cut, rate_cut, tables):
    real_rows, _, _, fore_cols, _, turn = tables
    narrow = rate_cut.shape[0]
    bands = (filter_in.shape[0] - 1) // 2
    units = filter_mid.shape[0]
    sigs = 2 * narrow
    pad_rows = -(-filter_in.shape[0] // 8) * 8
    w_in = jnp.pad(filter_in.T, ((0, 0), (0, pad_rows - filter_in.shape[0])))
    w_mid = filter_mid.T
    w_out = out_cut.transpose(1, 2, 3, 0).reshape(2, sigs, units)
    rates = jnp.broadcast_to(rate_cut[:, None], (narrow, LANES))
    full = 2 * length
    chunk = 2048
    steps = full // chunk
    sig_batch = min(4, sigs)
    rows = full // LANES
    whole = lambda shape: pl.BlockSpec(shape, lambda i: (0,) * len(shape))
    return pl.pallas_call(
        functools.partial(filter_kernel, bands, length, sig_batch, chunk, steps),
        grid=(steps + sigs // sig_batch,),
        in_specs=[
            whole(w_in.shape),
            whole(w_mid.shape),
            whole(w_out.shape),
            whole(rates.shape),
            whole(real_rows.shape),
            whole(fore_cols.shape),
            whole(turn.shape),
        ],
        out_specs=pl.BlockSpec(
            (sig_batch, rows, 2 * LANES), lambda i: (jnp.maximum(i - steps, 0), 0, 0)
        ),
        out_shape=jax.ShapeDtypeStruct((sigs, rows, 2 * LANES), f32),
        scratch_shapes=[
            pltpu.VMEM((rows * sigs, LANES), f32),
            pltpu.VMEM((sigs, LANES), f32),
        ],
        compiler_params=pltpu.CompilerParams(vmem_limit_bytes=56 * 2**20),
        cost_estimate=pl.CostEstimate(
            flops=30_000_000_000, bytes_accessed=sigs * rows * 1024, transcendentals=0
        ),
        name="filter_spectrum",
    )(w_in, w_mid, w_out, rates, real_rows, fore_cols, turn)


def conv_kernel(
    batch, x_ref, taps, gain, spec_ref, pair_ref, unpair_ref, fore_ref, back_ref, turn_ref,
    out0, out1, held, done
):
    i = pl.program_id(0)
    groups, pieces, narrow, tok_rows = x_ref.shape
    tiles = tok_rows // LANES
    rows = turn_ref.shape[1]

    @pl.when(i == 0)
    def _():
        lane = lax.broadcasted_iota(jnp.int32, (narrow, LANES), 1)
        for p in range(3):
            before, mid, after = taps[p], taps[3 + p], taps[6 + p]
            for s in range(2):
                ps = 2 * p + s

                def step(r, carry):
                    last = x_ref[jnp.maximum(r - 1, 0), ps, :, tok_rows - LANES :].astype(f32)
                    follow = x_ref[jnp.minimum(r + 1, groups - 1), ps, :, :LANES].astype(f32)
                    span = [last * jnp.where(r > 0, 1.0, 0.0)]
                    for j in range(tiles):
                        span.append(x_ref[r, ps, :, j * LANES : (j + 1) * LANES].astype(f32))
                    span.append(follow * jnp.where(r < groups - 1, 1.0, 0.0))
                    up = [pltpu.roll(v, 1, 1) for v in span[:-1]]
                    down = [pltpu.roll(v, LANES - 1, 1) for v in span[1:]]
                    for j in range(tiles):
                        prev = jnp.where(lane == 0, up[j], up[j + 1])
                        nxt = jnp.where(lane == LANES - 1, down[j + 1], down[j])
                        at = ((ps * groups + r) * tiles + j) * narrow
                        held[pl.ds(at, narrow), :] = before * prev + mid * span[j + 1] + after * nxt
                    return carry

                lax.fori_loop(0, groups, step, 0)

    c, s = turn_ref[0], turn_ref[1]
    first = i * batch

    def part(p, b):
        return held[pl.ds(p * rows * narrow + first + b, rows, stride=narrow), :]

    def lanes(v, b):
        return v[:, b * LANES : (b + 1) * LANES]

    carried = [part(0, b) for b in range(batch)]
    for o in range(2):
        z = jnp.concatenate([v.astype(bf16) for v in carried], axis=1)
        a = dot(pair_ref[0], z) + dot(pair_ref[1], z)
        turned = []
        for b in range(batch):
            ar, ai = lanes(a[:rows], b), lanes(a[rows:], b)
            turned.append(
                jnp.concatenate([(ar * c + ai * s).astype(bf16), (ai * c - ar * s).astype(bf16)], axis=1)
            )
        t = jnp.concatenate(turned, axis=0)
        spec = dot(t, fore_ref[0]) + dot(t, fore_ref[1])
        prods = []
        for b in range(batch):
            sr = spec[b * rows : (b + 1) * rows, :LANES]
            si = spec[b * rows : (b + 1) * rows, LANES:]
            kr = spec_ref[o, b, :, :LANES]
            ki = spec_ref[o, b, :, LANES:]
            prods.append(
                jnp.concatenate([(sr * kr - si * ki).astype(bf16), (sr * ki + si * kr).astype(bf16)], axis=1)
            )
        t = jnp.concatenate(prods, axis=0)
        g = dot(t, back_ref[0]) + dot(t, back_ref[1])
        turned = []
        for b in range(batch):
            gr = g[b * rows : (b + 1) * rows, :LANES]
            gi = g[b * rows : (b + 1) * rows, LANES:]
            turned.append(
                jnp.concatenate([(gr * c - gi * s).astype(bf16), (gi * c + gr * s).astype(bf16)], axis=0)
            )
        h = jnp.concatenate(turned, axis=1)
        y = dot(unpair_ref[0], h) + dot(unpair_ref[1], h)
        carried = [
            part(o + 1, b) * (lanes(y, b) + gain[o, first + b] * carried[b]) for b in range(batch)
        ]
    for b in range(batch):
        done[pl.ds(first + b, rows, stride=narrow), :] = carried[b]

    @pl.when(i == pl.num_programs(0) - 1)
    def _():
        for s_idx, out in enumerate((out0, out1)):

            def leave(r, carry):
                for j in range(tiles):
                    at = ((s_idx * groups + r) * tiles + j) * narrow
                    out[r, :, j * LANES : (j + 1) * LANES] = done[pl.ds(at, narrow), :].astype(bf16)
                return carry

            lax.fori_loop(0, groups, leave, 0)


def gated_conv(arrived, tap_cut, gain_cut, spectrum, tables):
    _, pair_rows, unpair_rows, fore_cols, back_cols, turn = tables
    groups, _, narrow, tok_rows = arrived.shape
    rows = turn.shape[1]
    batch = min(4, narrow)
    taps = jnp.broadcast_to(tap_cut.reshape(9, narrow)[:, :, None], (9, narrow, LANES))
    spectrum = spectrum.reshape(2, narrow, rows, 2 * LANES)
    whole = lambda shape: pl.BlockSpec(shape, lambda i: (0,) * len(shape))
    out = jax.ShapeDtypeStruct((groups, narrow, tok_rows), bf16)
    return pl.pallas_call(
        functools.partial(conv_kernel, batch),
        grid=(narrow // batch,),
        in_specs=[
            whole(arrived.shape),
            whole(taps.shape),
            pl.BlockSpec(memory_space=pltpu.SMEM),
            pl.BlockSpec((2, batch, rows, 2 * LANES), lambda i: (0, i, 0, 0)),
            whole(pair_rows.shape),
            whole(unpair_rows.shape),
            whole(fore_cols.shape),
            whole(back_cols.shape),
            whole(turn.shape),
        ],
        out_specs=[whole(out.shape), whole(out.shape)],
        out_shape=[out, out],
        scratch_shapes=[
            pltpu.VMEM((3 * rows * narrow, LANES), f32),
            pltpu.VMEM((rows * narrow, LANES), f32),
        ],
        compiler_params=pltpu.CompilerParams(vmem_limit_bytes=56 * 2**20),
        cost_estimate=pl.CostEstimate(
            flops=20_000_000_000, bytes_accessed=narrow * rows * 2048, transcendentals=0
        ),
        name="gated_conv",
    )(arrived, taps, gain_cut, spectrum, pair_rows, unpair_rows, fore_cols, back_cols, turn)


def on_device(
    tokens,
    w_value,
    w_first,
    w_second,
    short_taps,
    filter_in,
    filter_mid,
    filter_out,
    decay_rate,
    skip_gain,
    w_output,
):
    seq_count, tok_rows, _ = tokens.shape
    local_width = w_value.shape[1]
    groups = lax.axis_size("row")
    narrow = local_width // groups
    length = tok_rows * groups
    offset = lax.axis_index("row") * narrow
    tables = transform_tables(2 * length)
    projected = jnp.stack(
        [
            jnp.einsum("std,dc->sct", tokens, weight, preferred_element_type=f32).astype(bf16)
            for weight in (w_value, w_first, w_second)
        ]
    )
    projected = projected.reshape(3 * seq_count, groups, narrow, tok_rows).transpose(1, 0, 2, 3)
    arrived = lax.all_to_all(projected, "row", split_axis=0, concat_axis=0, tiled=True)
    tap_cut = lax.dynamic_slice_in_dim(short_taps, offset, narrow, 2)
    rate_cut = lax.dynamic_slice_in_dim(decay_rate, offset, narrow, 0)
    gain_cut = lax.dynamic_slice_in_dim(skip_gain, offset, narrow, 1)
    out_cut = lax.dynamic_slice_in_dim(filter_out, offset, narrow, 3)
    spectrum = make_spectrum(length, filter_in, filter_mid, out_cut, rate_cut, tables)
    gated = gated_conv(arrived, tap_cut, gain_cut, spectrum, tables)
    results = []
    for piece in gated:
        returned = lax.all_to_all(piece, "row", split_axis=0, concat_axis=0, tiled=True)
        returned = returned.reshape(local_width, tok_rows)
        gathered = lax.all_gather(returned, "col", axis=0, tiled=True)
        results.append(
            jnp.einsum("ct,cd->td", gathered, w_output, preferred_element_type=f32).astype(bf16)
        )
    return jnp.stack(results)


def solution(mesh):
    placed = (
        P(None, "row", None),
        P(None, "col"),
        P(None, "col"),
        P(None, "col"),
        P(None, None, "col"),
        P(),
        P(),
        P(None, None, None, "col"),
        P("col"),
        P(None, "col"),
        P(None, "col"),
    )
    return jax.shard_map(
        on_device, mesh=mesh, in_specs=placed, out_specs=P(None, "row", "col"), check_vma=False
    )
```

profile of v0, /device:TPU:15, one launch (start us, length us, event | category | flops | bytes accessed | tf_op | source)
XLA Modules:
  0.0 188.2 jit_solution(4973381180757246490)
XLA Ops:
  6.5 5.3 %fusion.21 = bf16[1,2,512,512]{3,2,1,0:T(8,128)(2,1)S(1)} fusion(bf16[2,512,2048]{2,1,0:T(8,128)(2,1)} %param.17, bf16[2048,512]{1,0:T(8,128)(2,1)} %param.18), kind=kOutput, calls=%fused_computation.16 | convolution fusion | flops 2148007936 | bytes 7340032 | tf_op jit(solution)/shard_map/std,dc->sct/dot_general | solution.py:337
  11.9 2.4 %fusion.18 = bf16[1,2,512,512]{3,2,1,0:T(8,128)(2,1)S(1)} fusion(bf16[2,512,2048]{2,1,0:T(8,128)(2,1)S(1)} %copy-done.3, bf16[2048,512]{1,0:T(8,128)(2,1)S(1)} %copy-done.4), kind=kOutput, calls=%fused_computation.15 | convolution fusion | flops 2148007936 | bytes 7340032 | tf_op jit(solution)/shard_map/std,dc->sct/dot_general | solution.py:337
  14.3 2.4 %fusion.15 = bf16[1,2,512,512]{3,2,1,0:T(8,128)(2,1)S(1)} fusion(bf16[2,512,2048]{2,1,0:T(8,128)(2,1)S(1)} %copy-done.3, bf16[2048,512]{1,0:T(8,128)(2,1)S(1)} %copy-done.5), kind=kOutput, calls=%fused_computation.14 | convolution fusion | flops 2148007936 | bytes 7340032 | tf_op jit(solution)/shard_map/std,dc->sct/dot_general | solution.py:337
  16.7 0.3 pad_maximum_fusion
  17.1 2.1 %copy.38 = bf16[6,16,32,512]{3,2,0,1:T(8,128)(2,1)} copy(bf16[6,16,32,512]{3,2,1,0:T(8,128)(2,1)S(1)} %bitcast.57) | data formatting | bytes 6291456 | tf_op jit(solution)/shard_map/reshape | solution.py:341
  19.2 6.7 %all-to-all-start = ((bf16[16,6,32,512]{3,2,1,0:T(8,128)(2,1)}), bf16[16,6,32,512]{3,2,1,0:T(8,128)(2,1)}, u32[]{:S(2)}, u32[]{:S(2)}) async-start(bf16[16,6,32,512]{3,2,1,0:T(8,128)(2,1)} %bitcast.56), calls=%async_computation | async-start | bytes 6291456 | tf_op jit(solution)/shard_map/all_to_all | solution.py:342
  26.2 0.8 dynamic_slice.15
  26.9 0.8 constant_dynamic-slice_fusion.1
  27.8 0.7 copy.29
  28.5 1.1 dynamic-slice_bitcast_fusion
  29.6 0.7 copy.30
  30.3 0.6 pad.4.w_in
  30.9 1.3 constant_dynamic-slice_fusion.gain
  32.3 0.7 broadcast_in_dim.15.rates
  33.0 33.4 %filter_spectrum.1 = f32[64,128,256]{2,1,0:T(8,128)} custom-call(f32[64,40]{1,0:T(8,128)} %pad.4.w_in, f32[64,64]{1,0:T(8,128)} %bitcast.62, f32[2,64,64]{2,1,0:T(8,128)} %bitcast.61, f32[32,128]{1,0:T(8,128)} %broadcast_in_dim.15.rates, bf16[2,256,128]{2,1,0:T(8,128)(2,1)} %constant.26.clone.rows_ref, ...), custom_call_target="tpu_custom_call" | custom-call | flops 30000001024 | bytes 8388608 | tf_op jit(solution)/shard_map/filter_spectrum/pallas_call | solution.py:155
  66.3 30.4 %all-to-all-done.x_ref = bf16[16,6,32,512]{3,2,1,0:T(8,128)(2,1)} async-done(((bf16[16,6,32,512]{3,2,1,0:T(8,128)(2,1)}), bf16[16,6,32,512]{3,2,1,0:T(8,128)(2,1)}, u32[]{:S(2)}, u32[]{:S(2)}) %all-to-all-start) | async-done | bytes 3145760 | tf_op jit(solution)/shard_map/all_to_all | solution.py:342
  96.7 0.8 broadcast_in_dim.14.taps
  97.5 33.3 %gated_conv.1 = (bf16[16,32,512]{2,1,0:T(8,128)(2,1)}, bf16[16,32,512]{2,1,0:T(8,128)(2,1)}) custom-call(bf16[16,6,32,512]{3,2,1,0:T(8,128)(2,1)} %all-to-all-done.x_ref, f32[9,32,128]{2,1,0:T(8,128)} %broadcast_in_dim.14.taps, f32[2,32]{1,0:T(2,128)} %constant_dynamic-slice_fusion.gain, f32[2,32,128,256]{3,2,1,0:T(8,128)} %bitcast.63, ...), custom_call_target="tpu_custom_call" | custom-call | flops 20000000000 | bytes 8388608 | tf_op jit(solution)/shard_map/gated_conv/pallas_call | solution.py:287
  130.8 17.2 %all_to_all.15 = bf16[16,32,512]{2,1,0:T(8,128)(2,1)} all-to-all(bf16[16,32,512]{2,1,0:T(8,128)(2,1)} %get-tuple-element.7), channel_id=1, replica_groups=mesh['row'=16,'col'=2] {'row'}, dimensions={0} | all-to-all | bytes 1048576 | tf_op jit(solution)/shard_map/all_to_all | solution.py:351
  148.1 18.4 %all_to_all.16 = bf16[16,32,512]{2,1,0:T(8,128)(2,1)} all-to-all(bf16[16,32,512]{2,1,0:T(8,128)(2,1)} %get-tuple-element.8), channel_id=1, replica_groups=mesh['row'=16,'col'=2] {'row'}, dimensions={0} | all-to-all | bytes 1048576 | tf_op jit(solution)/shard_map/all_to_all | solution.py:351
  166.5 2.5 %fusion.24 = bf16[1,512,1024]{2,1,0:T(8,128)(2,1)S(1)} fusion(bf16[1024,512]{1,0:T(8,128)(2,1)} %all-gather.3.cloned.1.call-done, bf16[1024,1024]{1,0:T(8,128)(2,1)S(1)} %copy-done), kind=kOutput, calls=%fused_computation.17 | convolution fusion | flops 1074266112 | bytes 4194304 | tf_op jit(solution)/shard_map/ct,cd->td/dot_general | solution.py:355
  169.0 8.3 %all-gather.5.cloned.1.call-done = bf16[1024,512]{1,0:T(8,128)(2,1)} async-done(((bf16[512,512]{1,0:T(8,128)(2,1)}), bf16[1024,512]{1,0:T(8,128)(2,1)}) %all-gather.5.cloned.1.call-update) | async-done | bytes 1048592 | tf_op jit(solution)/shard_map/all_gather | solution.py:353
  177.4 2.5 %fusion.25 = bf16[1,512,1024]{2,1,0:T(8,128)(2,1)S(1)} fusion(bf16[1024,512]{1,0:T(8,128)(2,1)} %all-gather.5.cloned.1.call-done, bf16[1024,1024]{1,0:T(8,128)(2,1)S(1)} %copy-done), kind=kOutput, calls=%fused_computation.18 | convolution fusion | flops 1074266112 | bytes 4194304 | tf_op jit(solution)/shard_map/ct,cd->td/dot_general | solution.py:355
  179.9 1.5 pad_maximum_fusion.1
  (19 shorter events, 0.4 us)
Async XLA Ops:
  6.5 160.0 %copy-start = (bf16[1024,1024]{1,0:T(8,128)(2,1)S(1)}, bf16[1024,1024]{1,0:T(8,128)(2,1)}, u32[]{:S(2)}) copy-start(bf16[1024,1024]{1,0:T(8,128)(2,1)} %param.27) | copy-start | bytes 6291460
  6.5 5.4 %copy-start.3 = (bf16[2,512,2048]{2,1,0:T(8,128)(2,1)S(1)}, bf16[2,512,2048]{2,1,0:T(8,128)(2,1)}, u32[]{:S(2)}) copy-start(bf16[2,512,2048]{2,1,0:T(8,128)(2,1)} %param.17) | copy-start | bytes 12582916
  6.5 5.4 %copy-start.4 = (bf16[2048,512]{1,0:T(8,128)(2,1)S(1)}, bf16[2048,512]{1,0:T(8,128)(2,1)}, u32[]{:S(2)}) copy-start(bf16[2048,512]{1,0:T(8,128)(2,1)} %param.19) | copy-start | bytes 6291460
  11.9 2.4 %copy-start.5 = (bf16[2048,512]{1,0:T(8,128)(2,1)S(1)}, bf16[2048,512]{1,0:T(8,128)(2,1)}, u32[]{:S(2)}) copy-start(bf16[2048,512]{1,0:T(8,128)(2,1)} %param.20) | copy-start | bytes 6291460
  19.2 8.5 %copy-start.2 = (f32[33,64]{1,0:T(8,128)S(1)}, f32[33,64]{1,0:T(8,128)}, u32[]{:S(2)}) copy-start(f32[33,64]{1,0:T(8,128)} %param.22) | copy-start | bytes 25348
  19.2 8.6 %copy-start.1 = (f32[64,64]{1,0:T(8,128)S(1)}, f32[64,64]{1,0:T(8,128)}, u32[]{:S(2)}) copy-start(f32[64,64]{1,0:T(8,128)} %param.23) | copy-start | bytes 49156
  19.2 77.5 %all-to-all-start = ((bf16[16,6,32,512]{3,2,1,0:T(8,128)(2,1)}), bf16[16,6,32,512]{3,2,1,0:T(8,128)(2,1)}, u32[]{:S(2)}, u32[]{:S(2)}) async-start(bf16[16,6,32,512]{3,2,1,0:T(8,128)(2,1)} %bitcast.56), calls=%async_computation | async-start | bytes 6291456 | tf_op jit(solution)/shard_map/all_to_all | solution.py:342
  25.9 140.6 %all-gather.3.cloned.1.call-start = ((), (), s32[]{:S(2)}) async-start(), calls=%async_computation.3 | async-start | bytes 1572864 | tf_op jit(solution)/shard_map/all_gather | solution.py:353
  148.0 29.3 %all-gather.5.cloned.1.call-start = ((), (), s32[]{:S(2)}) async-start(), calls=%async_computation.4 | async-start | bytes 1572864 | tf_op jit(solution)/shard_map/all_gather | solution.py:353
Sparse Core Ops, SparseCore 0:
  148.2 10.7 all-gather.2
  166.6 10.7 all-gather.4
where the time goes:
time: 190 us; the launch traced here: 188 us
  Pallas kernels  66.7 us (35%)
  waiting for transfers between devices  38.8 us (20%)
  blocking collectives  35.6 us (19%)
  matrix products  15.1 us (8%)
  between operations  13.5 us (7%)
  local copies, waits for them, and re-layouts  9.71 us (5%)
  starting transfers between devices  6.97 us (4%)
    all_to_all x2, blocking collectives, on_device(): lax.all_to_all(piece, 'row', split_axis=0, concat_axis=0, tiled=True)  35.6 us
    pallas_call x1, Pallas kernels, make_spectrum(): pl.pallas_call(functools.partial(filter_kernel, bands, length, sig_batch,...  33.4 us
    pallas_call x1, Pallas kernels, gated_conv(): pl.pallas_call(functools.partial(conv_kernel, batch), grid=(narrow // bat...  33.3 us
    all_to_all x1, waiting for transfers between devices, on_device(): lax.all_to_all(projected, 'row', split_axis=0, concat_axis=0, tiled=True)  30.4 us
    dot_general x3, matrix products, on_device(): jnp.einsum('std,dc->sct', tokens, weight, preferred_element_type=f32)  10.1 us
    all_gather x2, waiting for transfers between devices, on_device(): gathered = lax.all_gather(returned, 'col', axis=0, tiled=True)  8.37 us
    all_to_all x1, starting transfers between devices, on_device(): lax.all_to_all(projected, 'row', split_axis=0, concat_axis=0, tiled=True)  6.71 us
    dot_general x2, matrix products, on_device(): jnp.einsum('ct,cd->td', gathered, w_output, preferred_element_type=f32)  4.98 us
  transfers between devices with their start and end apart: 3, of which 2 were waited for; matrix products, arithmetic and copies ran while one was open for 5% of the time, Pallas kernels for 18%

commit v1 on v0

--- a/solution.py
+++ b/solution.py
@@ -182,7 +182,7 @@
 
 def conv_kernel(
     batch, x_ref, taps, gain, spec_ref, pair_ref, unpair_ref, fore_ref, back_ref, turn_ref,
-    out0, out1, held, done
+    out, held, done
 ):
     i = pl.program_id(0)
     groups, pieces, narrow, tok_rows = x_ref.shape
@@ -264,12 +264,12 @@
 
     @pl.when(i == pl.num_programs(0) - 1)
     def _():
-        for s_idx, out in enumerate((out0, out1)):
+        for s_idx in range(2):
 
             def leave(r, carry):
                 for j in range(tiles):
                     at = ((s_idx * groups + r) * tiles + j) * narrow
-                    out[r, :, j * LANES : (j + 1) * LANES] = done[pl.ds(at, narrow), :].astype(bf16)
+                    out[r, s_idx, :, j * LANES : (j + 1) * LANES] = done[pl.ds(at, narrow), :].astype(bf16)
                 return carry
 
             lax.fori_loop(0, groups, leave, 0)
@@ -283,7 +283,7 @@
     taps = jnp.broadcast_to(tap_cut.reshape(9, narrow)[:, :, None], (9, narrow, LANES))
     spectrum = spectrum.reshape(2, narrow, rows, 2 * LANES)
     whole = lambda shape: pl.BlockSpec(shape, lambda i: (0,) * len(shape))
-    out = jax.ShapeDtypeStruct((groups, narrow, tok_rows), bf16)
+    out = jax.ShapeDtypeStruct((groups, 2, narrow, tok_rows), bf16)
     return pl.pallas_call(
         functools.partial(conv_kernel, batch),
         grid=(narrow // batch,),
@@ -298,8 +298,8 @@
             whole(back_cols.shape),
             whole(turn.shape),
         ],
-        out_specs=[whole(out.shape), whole(out.shape)],
-        out_shape=[out, out],
+        out_specs=whole(out.shape),
+        out_shape=out,
         scratch_shapes=[
             pltpu.VMEM((3 * rows * narrow, LANES), f32),
             pltpu.VMEM((rows * narrow, LANES), f32),
@@ -310,6 +310,82 @@
         ),
         name="gated_conv",
     )(arrived, taps, gain_cut, spectrum, pair_rows, unpair_rows, fore_cols, back_cols, turn)
+
+
+def return_kernel(groups, x, out, own, own_sem, send_sem, recv_sem, pass_sem, take_sem):
+    me = lax.axis_index("row")
+    side = lax.axis_index("col")
+    mesh_ids = pl.DeviceIdType.MESH
+    barrier = pltpu.get_barrier_semaphore()
+    for k in range(1, groups):
+        peer = lax.rem(me + k, groups)
+        pl.semaphore_signal(barrier, inc=1, device_id=(peer, side), device_id_type=mesh_ids)
+    pl.semaphore_signal(barrier, inc=1, device_id=(me, 1 - side), device_id_type=mesh_ids)
+    pl.semaphore_wait(barrier, groups)
+
+    sends = []
+    for k in range(1, groups):
+        peer = lax.rem(me + k, groups)
+        sends.append(
+            pltpu.make_async_remote_copy(
+                src_ref=x.at[peer],
+                dst_ref=out.at[:, side, me],
+                send_sem=send_sem.at[k],
+                recv_sem=recv_sem.at[k],
+                device_id=(peer, side),
+                device_id_type=mesh_ids,
+            )
+        )
+        sends[-1].start()
+
+    def hand_over(k, source, place):
+        copy = pltpu.make_async_remote_copy(
+            src_ref=source,
+            dst_ref=out.at[:, side, place],
+            send_sem=pass_sem.at[k],
+            recv_sem=take_sem.at[k],
+            device_id=(me, 1 - side),
+            device_id_type=mesh_ids,
+        )
+        copy.start()
+        return copy
+
+    passes = [hand_over(0, x.at[me], me)]
+    fetch = pltpu.make_async_copy(x.at[me], own, own_sem.at[0])
+    fetch.start()
+    fetch.wait()
+    keep = pltpu.make_async_copy(own, out.at[:, side, me], own_sem.at[1])
+    keep.start()
+    for k in range(1, groups):
+        sends[k - 1].wait_recv()
+        source = lax.rem(me + groups - k, groups)
+        passes.append(hand_over(k, out.at[:, side, source], source))
+    keep.wait()
+    for copy in sends:
+        copy.wait_send()
+    for copy in passes:
+        copy.wait()
+
+
+def return_blocks(gated):
+    groups, seqs, narrow, tok_rows = gated.shape
+    out = pl.pallas_call(
+        functools.partial(return_kernel, groups),
+        in_specs=[pl.BlockSpec(memory_space=pl.ANY)],
+        out_specs=pl.BlockSpec(memory_space=pl.ANY),
+        out_shape=jax.ShapeDtypeStruct((seqs, 2, groups, narrow, tok_rows), bf16),
+        scratch_shapes=[
+            pltpu.VMEM((seqs, narrow, tok_rows), bf16),
+            pltpu.SemaphoreType.DMA((2,)),
+            pltpu.SemaphoreType.DMA((groups,)),
+            pltpu.SemaphoreType.DMA((groups,)),
+            pltpu.SemaphoreType.DMA((groups,)),
+            pltpu.SemaphoreType.DMA((groups,)),
+        ],
+        compiler_params=pltpu.CompilerParams(collective_id=0, has_side_effects=True),
+        name="return_blocks",
+    )(gated)
+    return out.reshape(seqs, 2 * groups * narrow, tok_rows)
 
 
 def on_device(
@@ -346,15 +422,14 @@
     out_cut = lax.dynamic_slice_in_dim(filter_out, offset, narrow, 3)
     spectrum = make_spectrum(length, filter_in, filter_mid, out_cut, rate_cut, tables)
     gated = gated_conv(arrived, tap_cut, gain_cut, spectrum, tables)
-    results = []
-    for piece in gated:
-        returned = lax.all_to_all(piece, "row", split_axis=0, concat_axis=0, tiled=True)
-        returned = returned.reshape(local_width, tok_rows)
-        gathered = lax.all_gather(returned, "col", axis=0, tiled=True)
-        results.append(
-            jnp.einsum("ct,cd->td", gathered, w_output, preferred_element_type=f32).astype(bf16)
-        )
-    return jnp.stack(results)
+    if groups <= 16 and lax.axis_size("col") == 2:
+        gathered = return_blocks(gated)
+    else:
+        returned = lax.all_to_all(gated, "row", split_axis=0, concat_axis=0, tiled=True)
+        returned = returned.transpose(1, 0, 2, 3).reshape(seq_count, local_width, tok_rows)
+        gathered = lax.all_gather(returned, "col", axis=1, tiled=True)
+    result = jnp.einsum("sct,cd->std", gathered, w_output, preferred_element_type=f32)
+    return result.astype(bf16)
 
 
 def solution(mesh):

time: 190 us -> 160 us (0.84)
  blocking collectives: 35.6 us -> 0 us
  Pallas kernels: 66.7 us -> 96.2 us
  between operations: 13.5 us -> 0.1 us
  waiting for transfers between devices: 38.8 us -> 30.7 us
    all_to_all x2 -> x0, blocking collectives: 35.6 us -> none  [on_device(): lax.all_to_all(piece, 'row', split_axis=0, concat_axis=0, tiled=True)]
    pallas_call x0 -> x1, Pallas kernels: none -> 29.6 us  [return_blocks(): pl.pallas_call(functools.partial(return_kernel, groups), in_specs=[pl.Blo...]
    all_gather x2 -> x0, waiting for transfers between devices: 8.37 us -> none  [on_device(): gathered = lax.all_gather(returned, 'col', axis=0, tiled=True)]
    dot_general x2 -> x1, matrix products: 4.98 us -> 5.29 us  [on_device(): jnp.einsum('sct,cd->std', gathered, w_output, preferred_element_type=f32)]
  transfers between devices with their start and end apart: 3 -> 1, of which waited for: 2 -> 1; matrix products, arithmetic and copies ran while one was open for 5% -> 4% of each run, Pallas kernels for 18% -> 21%
where the time goes in v1:
time: 160 us; the launch traced here: 159 us
  Pallas kernels  96.2 us (60%)
  waiting for transfers between devices  30.7 us (19%)
  matrix products  15.4 us (10%)
  local copies, waits for them, and re-layouts  9.69 us (6%)
  starting transfers between devices  6.71 us (4%)
    pallas_call x1, Pallas kernels, make_spectrum(): pl.pallas_call(functools.partial(filter_kernel, bands, length, sig_batch,...  33.4 us
    pallas_call x1, Pallas kernels, gated_conv(): pl.pallas_call(functools.partial(conv_kernel, batch), grid=(narrow // bat...  33.3 us
    all_to_all x1, waiting for transfers between devices, on_device(): lax.all_to_all(projected, 'row', split_axis=0, concat_axis=0, tiled=True)  30.7 us
    pallas_call x1, Pallas kernels, return_blocks(): pl.pallas_call(functools.partial(return_kernel, groups), in_specs=[pl.Blo...  29.6 us
    dot_general x3, matrix products, on_device(): jnp.einsum('std,dc->sct', tokens, weight, preferred_element_type=f32)  10.1 us
    all_to_all x1, starting transfers between devices, on_device(): lax.all_to_all(projected, 'row', split_axis=0, concat_axis=0, tiled=True)  6.71 us
    dot_general x1, matrix products, on_device(): jnp.einsum('sct,cd->std', gathered, w_output, preferred_element_type=f32)  5.29 us
  transfers between devices with their start and end apart: 1, of which 1 were waited for; matrix products, arithmetic and copies ran while one was open for 4% of the time, Pallas kernels for 21%

profile of v1, /device:TPU:15, one launch (start us, length us, event | category | flops | bytes accessed | tf_op | source)
XLA Modules:
  0.0 159.1 jit_solution(6870483649855624386)
XLA Ops:
  0.0 0.0 copy-start
  0.0 5.3 %fusion.26 = bf16[1,2,512,512]{3,2,1,0:T(8,128)(2,1)S(1)} fusion(bf16[2,512,2048]{2,1,0:T(8,128)(2,1)} %param.17, bf16[2048,512]{1,0:T(8,128)(2,1)} %param.18), kind=kOutput, calls=%fused_computation.16 | convolution fusion | flops 2148007936 | bytes 7340032 | tf_op jit(solution)/shard_map/std,dc->sct/dot_general | solution.py:413
  5.4 0.0 copy-done.3
  5.4 0.0 copy-start.5
  5.4 2.4 %fusion.23 = bf16[1,2,512,512]{3,2,1,0:T(8,128)(2,1)S(1)} fusion(bf16[2,512,2048]{2,1,0:T(8,128)(2,1)S(1)} %copy-done.3, bf16[2048,512]{1,0:T(8,128)(2,1)S(1)} %copy-done.4), kind=kOutput, calls=%fused_computation.15 | convolution fusion | flops 2148007936 | bytes 7340032 | tf_op jit(solution)/shard_map/std,dc->sct/dot_general | solution.py:413
  7.8 2.4 %fusion.20 = bf16[1,2,512,512]{3,2,1,0:T(8,128)(2,1)S(1)} fusion(bf16[2,512,2048]{2,1,0:T(8,128)(2,1)S(1)} %copy-done.3, bf16[2048,512]{1,0:T(8,128)(2,1)S(1)} %copy-done.5), kind=kOutput, calls=%fused_computation.14 | convolution fusion | flops 2148007936 | bytes 7340032 | tf_op jit(solution)/shard_map/std,dc->sct/dot_general | solution.py:413
  10.2 0.3 pad_maximum_fusion
  10.5 2.1 %copy.41 = bf16[6,16,32,512]{3,2,0,1:T(8,128)(2,1)} copy(bf16[6,16,32,512]{3,2,1,0:T(8,128)(2,1)S(1)} %bitcast.54) | data formatting | bytes 6291456 | tf_op jit(solution)/shard_map/reshape | solution.py:417
  12.7 6.7 %all-to-all-start = ((bf16[16,6,32,512]{3,2,1,0:T(8,128)(2,1)}), bf16[16,6,32,512]{3,2,1,0:T(8,128)(2,1)}, u32[]{:S(2)}, u32[]{:S(2)}) async-start(bf16[16,6,32,512]{3,2,1,0:T(8,128)(2,1)} %bitcast.53), calls=%async_computation | async-start | bytes 6291456 | tf_op jit(solution)/shard_map/all_to_all | solution.py:418
  19.4 0.8 dynamic_slice.15
  20.1 0.8 constant_dynamic-slice_fusion.1
  20.9 0.1 copy.29
  21.0 0.7 copy.30
  21.7 1.1 dynamic-slice_bitcast_fusion
  22.8 0.7 copy.31
  23.6 0.6 pad.4.w_in
  24.2 1.3 constant_dynamic-slice_fusion.gain
  25.5 0.7 broadcast_in_dim.15.rates
  26.2 33.4 %filter_spectrum.1 = f32[64,128,256]{2,1,0:T(8,128)} custom-call(f32[64,40]{1,0:T(8,128)} %pad.4.w_in, f32[64,64]{1,0:T(8,128)} %bitcast.58, f32[2,64,64]{2,1,0:T(8,128)} %bitcast.57, f32[32,128]{1,0:T(8,128)} %broadcast_in_dim.15.rates, bf16[2,256,128]{2,1,0:T(8,128)(2,1)} %constant.26.clone.rows_ref, ...), custom_call_target="tpu_custom_call" | custom-call | flops 30000001024 | bytes 8388608 | tf_op jit(solution)/shard_map/filter_spectrum/pallas_call | solution.py:155
  59.5 30.7 %all-to-all-done.x_ref = bf16[16,6,32,512]{3,2,1,0:T(8,128)(2,1)} async-done(((bf16[16,6,32,512]{3,2,1,0:T(8,128)(2,1)}), bf16[16,6,32,512]{3,2,1,0:T(8,128)(2,1)}, u32[]{:S(2)}, u32[]{:S(2)}) %all-to-all-start) | async-done | bytes 3145760 | tf_op jit(solution)/shard_map/all_to_all | solution.py:418
  90.2 0.8 broadcast_in_dim.14.taps
  91.0 33.3 %gated_conv.1.x = bf16[16,2,32,512]{3,2,1,0:T(8,128)(2,1)} custom-call(bf16[16,6,32,512]{3,2,1,0:T(8,128)(2,1)} %all-to-all-done.x_ref, f32[9,32,128]{2,1,0:T(8,128)} %broadcast_in_dim.14.taps, f32[2,32]{1,0:T(2,128)} %constant_dynamic-slice_fusion.gain, f32[2,32,128,256]{3,2,1,0:T(8,128)} %bitcast.59, bf16[2,256,128]{2,1,0:T(8,128)(2,1)} %constant.29.clone.pair_ref, ...), custom_call_target="tpu_custom_call" | custom-call | flops 20000000000 | bytes 8388608 | tf_op jit(solution)/shard_map/gated_conv/pallas_call | solution.py:287
  124.3 29.6 %return_blocks.1 = bf16[2,2,16,32,512]{4,3,2,1,0:T(8,128)(2,1)} custom-call(bf16[16,2,32,512]{3,2,1,0:T(8,128)(2,1)} %gated_conv.1.x), custom_call_target="tpu_custom_call" | custom-call | tf_op jit(solution)/shard_map/return_blocks/pallas_call | solution.py:372
  153.8 5.3 %fusion.8 = bf16[2,512,1024]{2,1,0:T(8,128)(2,1)} fusion(bf16[2,1024,512]{2,1,0:T(8,128)(2,1)} %bitcast.55, bf16[1024,1024]{1,0:T(8,128)(2,1)S(1)} %copy-done), kind=kOutput, calls=%fused_computation.10 | convolution fusion | flops 2148532224 | bytes 6291456 | tf_op jit(solution)/shard_map/sct,cd->std/dot_general | solution.py:431
  (10 shorter events, 0.0 us)
Async XLA Ops:
  0.0 153.8 %copy-start = (bf16[1024,1024]{1,0:T(8,128)(2,1)S(1)}, bf16[1024,1024]{1,0:T(8,128)(2,1)}, u32[]{:S(2)}) copy-start(bf16[1024,1024]{1,0:T(8,128)(2,1)} %param.27) | copy-start | bytes 6291460
  0.0 5.4 %copy-start.3 = (bf16[2,512,2048]{2,1,0:T(8,128)(2,1)S(1)}, bf16[2,512,2048]{2,1,0:T(8,128)(2,1)}, u32[]{:S(2)}) copy-start(bf16[2,512,2048]{2,1,0:T(8,128)(2,1)} %param.17) | copy-start | bytes 12582916
  0.0 5.4 %copy-start.4 = (bf16[2048,512]{1,0:T(8,128)(2,1)S(1)}, bf16[2048,512]{1,0:T(8,128)(2,1)}, u32[]{:S(2)}) copy-start(bf16[2048,512]{1,0:T(8,128)(2,1)} %param.19) | copy-start | bytes 6291460
  5.4 2.4 %copy-start.5 = (bf16[2048,512]{1,0:T(8,128)(2,1)S(1)}, bf16[2048,512]{1,0:T(8,128)(2,1)}, u32[]{:S(2)}) copy-start(bf16[2048,512]{1,0:T(8,128)(2,1)} %param.20) | copy-start | bytes 6291460
  12.7 8.2 %copy-start.2 = (f32[33,64]{1,0:T(8,128)S(1)}, f32[33,64]{1,0:T(8,128)}, u32[]{:S(2)}) copy-start(f32[33,64]{1,0:T(8,128)} %param.22) | copy-start | bytes 25348
  12.7 8.3 %copy-start.1 = (f32[64,64]{1,0:T(8,128)S(1)}, f32[64,64]{1,0:T(8,128)}, u32[]{:S(2)}) copy-start(f32[64,64]{1,0:T(8,128)} %param.23) | copy-start | bytes 49156
  12.7 77.5 %all-to-all-start = ((bf16[16,6,32,512]{3,2,1,0:T(8,128)(2,1)}), bf16[16,6,32,512]{3,2,1,0:T(8,128)(2,1)}, u32[]{:S(2)}, u32[]{:S(2)}) async-start(bf16[16,6,32,512]{3,2,1,0:T(8,128)(2,1)} %bitcast.53), calls=%async_computation | async-start | bytes 6291456 | tf_op jit(solution)/shard_map/all_to_all | solution.py:418
